TPU v7x, 128 devices: a whole 4x4x4 slice. The times are simulated.
128 devices in a mesh: rep: 2 (over z_hi), fs: 32 (over z_lo, y, x), tp: 2 (over core).
Axes of the slice: x: 4, y: 4, z: 4 (z_hi: 2, z_lo: 2; z = z_hi * 2 + z_lo), core: 2. Of those that a mesh axis runs over, the one named last changes fastest.
Arguments:
- tokens: bfloat16 [65536, 2048], P(('rep', 'fs')), may hold values from -6 to 6
- norm_mix: bfloat16 [2048], replicated, may hold values from 0.099609375 to 1.8984375
- w_unit: bfloat16 [2048, 1024], P('fs', 'tp'), may hold values from -0.125 to 0.125
- w_value: bfloat16 [2048, 1024], P('fs', 'tp'), may hold values from -0.125 to 0.125
- spatial: bfloat16 [4, 128, 128], replicated, may hold values from -0.52734375 to 0.52734375
- spatial_bias: bfloat16 [4, 128], replicated, may hold values from 0.099609375 to 1.8984375
- group_gain: bfloat16 [1024], replicated, may hold values from 0.099609375 to 1.8984375
- group_shift: bfloat16 [1024], replicated, may hold values from -3 to 3
- w_mix_out: bfloat16 [1024, 2048], P('tp', 'fs'), may hold values from -0.1875 to 0.1875
- norm_ffn: bfloat16 [2048], replicated, may hold values from 0.099609375 to 1.8984375
- w_gate: bfloat16 [2048, 2816], P('fs', 'tp'), may hold values from -0.125 to 0.125
- w_up: bfloat16 [2048, 2816], P('fs', 'tp'), may hold values from -0.125 to 0.125
- w_down: bfloat16 [2816, 2048], P('tp', 'fs'), may hold values from -0.109375 to 0.109375
Outputs:
- layer_out: bfloat16 [65536, 2048], P(('rep', 'fs', 'tp'))
All inputs are finite; a program needn't handle non-finite values.
Results may differ from a plain program's by a relative error of at most 0.008.
Values may be sent and summed in bfloat16 or wider, within the bound.
No kernel may reach another device: no remote copies, remote signals or barrier semaphores. Data moves between devices by JAX's collectives and lax.ppermute only.
A program may use at most 128 MiB of HBM per device.

v0:
```python
import jax
import jax.numpy as jnp
from jax import lax
from jax.sharding import PartitionSpec as P


def sent_together(arrays, axis, dim, along):
    ends, at = ([], 0)
    for a in arrays[:-1]:
        at += a.shape[along]
        ends.append(at)
    both = jnp.concatenate(arrays, axis=along)
    return tuple(jnp.split(lax.all_gather(both, axis, axis=dim, tiled=True), ends, axis=along))


def sent_to_all(x, axis):
    copies = jnp.broadcast_to(x, (lax.axis_size(axis), *x.shape))
    return lax.all_to_all(copies, axis, split_axis=0, concat_axis=0, tiled=True)


def in_order(pieces, dim):
    pieces = jnp.moveaxis(pieces, 0, dim)
    dims = pieces.shape
    return pieces.reshape(*dims[:dim], dims[dim] * dims[dim + 1], *dims[dim + 2 :])


def gathered_copies(x, axis, dim):
    pieces = sent_to_all(x, axis)
    return in_order(pieces, dim)


def total_of_pieces(x, axis):
    return lax.all_gather(x, axis).sum(0)


def split_up(x, dim, peers):
    before, after = (x.shape[:dim], x.shape[dim + 1 :])
    return jnp.moveaxis(x.reshape(*before, peers, -1, *after), dim, 0)


def summed_on_arrival(x, axis, dim):
    pieces = split_up(x, dim, lax.axis_size(axis))
    arrived = lax.all_to_all(pieces, axis, split_axis=0, concat_axis=0, tiled=True)
    return arrived.astype(jnp.float32).sum(axis=0)


def rms_scale(values, gain):
    values = values.astype(jnp.float32)
    scale = lax.rsqrt(jnp.mean(values * values, axis=-1, keepdims=True) + 1e-06)
    return values * scale * gain.astype(jnp.float32)


def spatial_unit(unit_pre, value_pre, spatial, spatial_bias, group_gain, group_shift):
    count, width = value_pre.shape
    groups = spatial.shape[0]
    block = spatial.shape[1]
    active = jax.nn.gelu(value_pre, approximate=True).reshape(count, groups, width // groups)
    center = jnp.mean(active, axis=-1, keepdims=True)
    spread = jnp.mean(jnp.square(active - center), axis=-1, keepdims=True)
    normal = ((active - center) * lax.rsqrt(spread + 1e-06)).reshape(count, width)
    normal = normal * group_gain.astype(jnp.float32) + group_shift.astype(jnp.float32)
    grouped = normal.astype(jnp.bfloat16)
    causal = jnp.tril(jnp.ones((block, block), dtype=bool))
    weights = jnp.where(causal[None], spatial, jnp.zeros_like(spatial))
    tiles = grouped.reshape(count // block, block, groups, width // groups)
    mixed = jnp.einsum("gts,nsgd->ntgd", weights, tiles, preferred_element_type=jnp.float32)
    mixed = mixed + spatial_bias.astype(jnp.float32).T[None, :, :, None]
    return jax.nn.gelu(unit_pre, approximate=True) * mixed.reshape(count, width)


def on_device(
    tokens,
    norm_mix,
    w_unit,
    w_value,
    spatial,
    spatial_bias,
    group_gain,
    group_shift,
    w_mix_out,
    norm_ffn,
    w_gate,
    w_up,
    w_down,
):
    count = tokens.shape[0]
    half = count // lax.axis_size("tp")
    position = lax.axis_index("tp")
    row_start = position * half
    local_width = w_unit.shape[1]
    group_count = spatial.shape[0] // lax.axis_size("tp")
    group_start = position * group_count
    spatial_local = lax.dynamic_slice_in_dim(spatial, group_start, group_count, 0)
    bias_local = lax.dynamic_slice_in_dim(spatial_bias, group_start, group_count, 0)
    gain_local = lax.dynamic_slice_in_dim(group_gain, position * local_width, local_width, 0)
    shift_local = lax.dynamic_slice_in_dim(group_shift, position * local_width, local_width, 0)
    normed = rms_scale(tokens, norm_mix).astype(jnp.bfloat16)
    unit_whole, value_whole = sent_together((w_unit, w_value), "fs", 0, 1)
    unit_pre = jnp.dot(normed, unit_whole, preferred_element_type=jnp.float32)
    value_pre = jnp.dot(normed, value_whole, preferred_element_type=jnp.float32)
    gated = spatial_unit(
        unit_pre, value_pre, spatial_local, bias_local, gain_local, shift_local
    ).astype(jnp.bfloat16)
    partial_terms = jnp.dot(
        gated, gathered_copies(w_mix_out, "fs", 1), preferred_element_type=jnp.float32
    )
    summed = total_of_pieces(partial_terms, "tp")
    h_mid = (tokens.astype(jnp.float32) + summed).astype(jnp.bfloat16)
    normed_mid = rms_scale(h_mid, norm_ffn).astype(jnp.bfloat16)
    gate_whole, up_whole = sent_together((w_gate, w_up), "fs", 0, 1)
    gate = jnp.dot(normed_mid, gate_whole, preferred_element_type=jnp.float32)
    up = jnp.dot(normed_mid, up_whole, preferred_element_type=jnp.float32)
    hidden = (jax.nn.silu(gate) * up).astype(jnp.bfloat16)
    down_cols = lax.all_gather(w_down, "fs", axis=1, tiled=True)
    residual_rows = lax.dynamic_slice_in_dim(h_mid, row_start, half, 0).astype(jnp.float32)
    summed_rows = summed_on_arrival(
        jnp.dot(hidden, down_cols, preferred_element_type=jnp.float32).astype(jnp.bfloat16), "tp", 0
    )
    return (residual_rows + summed_rows).astype(jnp.bfloat16)


def solution(mesh):
    placed = (
        P(("rep", "fs"), None),
        P(),
        P("fs", "tp"),
        P("fs", "tp"),
        P(),
        P(),
        P(),
        P(),
        P("tp", "fs"),
        P(),
        P("fs", "tp"),
        P("fs", "tp"),
        P("tp", "fs"),
    )
    return jax.shard_map(
        on_device,
        mesh=mesh,
        in_specs=placed,
        out_specs=P(("rep", "fs", "tp"), None),
        check_vma=False,
    )
```

profile of v0, /device:TPU:1, one launch (start us, length us, event | category | flops | bytes accessed | tf_op | source)
XLA Modules:
  0.0 629.2 jit_solution(16438548954573870074)
XLA Ops:
  6.5 0.0 all-gather.6.cloned.1.call-start
  6.6 1.6 pad_maximum_fusion.1
  8.1 0.0 all-gather.6.cloned.1.call-update
  8.2 2.4 broadcast_in_dim.13
  10.6 9.3 %all-to-all-start = ((bf16[32,512,64]{1,2,0:T(8,128)(2,1)}), bf16[32,512,64]{1,2,0:T(8,128)(2,1)}, u32[]{:S(2)}, u32[]{:S(2)}) async-start(bf16[32,512,64]{1,2,0:T(8,128)(2,1)} %broadcast_in_dim.13), calls=%async_computation | async-start | bytes 4194304 | tf_op jit(solution)/shard_map/all_to_all | solution.py:18
  19.9 0.0 all-gather.12.cloned.1.call-start
  20.0 0.0 copy-done.5
  20.0 0.0 copy-done.9
  20.0 0.0 copy-done.8
  20.0 0.1 dynamic-slice_convert_fusion
  20.1 3.1 fusion.3
  23.3 133.9 %all-gather.6.cloned.1.call-done = bf16[2048,1024]{1,0:T(8,128)(2,1)} async-done(((bf16[64,1024]{1,0:T(8,128)(2,1)}), bf16[2048,1024]{1,0:T(8,128)(2,1)}) %all-gather.6.cloned.1.call-update) | async-done | bytes 4194320 | tf_op jit(solution)/shard_map/all_gather | solution.py:13
  157.1 6.9 %fusion.35 = f32[1024,512]{1,0:T(8,128)} fusion(bf16[2048,1024]{1,0:T(8,128)(2,1)} %all-gather.6.cloned.1.call-done, bf16[1024,2048]{1,0:T(8,128)(2,1)} %param.13, f32[2048]{0:T(1024)S(1)} %convert_element_type.51, f32[1024]{0:T(1024)S(1)} %add_rsqrt_fusion.2), kind=kOutput, calls=%fused_computation.39 | convolution fusion | flops 2160066560 | bytes 8400896 | tf_op jit(solution)/shard_map/dot_general | solution.py:100
  164.1 2.6 reshape.58
  166.7 1.2 reduce_sum.55
  167.9 14.4 %multiply_reduce_fusion = f32[1024,2]{1,0:T(8,128)S(1)} fusion(f32[1024,2,256]{2,1,0:T(2,128)S(1)} %reshape.58, f32[1024,2]{1,0:T(8,128)S(1)} %broadcast_multiply_fusion), kind=kLoop, calls=%fused_computation.46 | loop fusion | flops 1570816 | bytes 2113536 | tf_op jit(solution)/shard_map/reduce_sum | solution.py:59
  182.3 0.1 add_rsqrt_fusion
  182.4 1.2 mul.112
  183.6 0.2 copy.32
  183.8 1.2 sub.17
  185.1 0.2 copy.31
  185.3 0.2 copy-done.1
  185.4 0.8 add_convert_fusion.1
  186.2 0.3 reshape.59
  186.5 0.5 bitcast_add_fusion
  187.1 2.4 copy.28
  189.5 1.8 copy.33
  191.2 0.0 all-to-all-done
  191.3 11.6 %fusion.51 = f32[1024,2048]{1,0:T(8,128)} fusion(bf16[512,2048]{0,1:T(8,128)(2,1)} %bitcast.5, f32[1024,512]{1,0:T(8,128)S(1)} %bitcast.30, bf16[2048,1024]{1,0:T(8,128)(2,1)} %all-gather.6.cloned.1.call-done, bf16[1024,2048]{1,0:T(8,128)(2,1)} %param.13, f32[2048]{0:T(1024)S(1)} %convert_element_type.51, f32[1024]{0:T(1024)S(1)} %add_rsqrt_fusion.2), kind=kOutput, calls=%fused_computation.47 | convolution fusion | flops 4308598784 | bytes 18886656 | tf_op jit(solution)/shard_map/dot_general | solution.py:104
  202.9 0.0 all-gather.12.cloned.1.call-update
  202.9 0.0 all-gather.8.cloned.1.call-start
  203.0 0.8 copy-done.2
  203.8 0.1 copy-done.3
  203.9 0.8 pad_maximum_fusion
  204.6 0.0 all-gather.8.cloned.1.call-update
  204.7 0.0 all-gather.10.cloned.1.call-start
  204.7 0.5 all-gather.10.cloned.1.call-update
  205.3 49.1 %all-gather.12.cloned.1.call-done = f32[2048,2048]{1,0:T(8,128)} async-done(((f32[1024,2048]{1,0:T(8,128)}), f32[2048,2048]{1,0:T(8,128)}) %all-gather.12.cloned.1.call-update) | async-done | bytes 16777232 | tf_op jit(solution)/shard_map/all_gather | solution.py:33
  254.4 11.8 %reduce_sum.57 = f32[1024,2048]{1,0:T(8,128)} reduce(f32[2,1024,2048]{2,1,0:T(8,128)} %bitcast.23, f32[]{:T(128)} %constant.15.clone.1), dimensions={0}, to_apply=%region_3.4 | reduce | flops 2097152 | bytes 25165828 | tf_op jit(solution)/shard_map/reduce_sum | solution.py:33
  266.1 7.8 %fusion = (f32[1024]{0:T(1024)S(1)}, bf16[1024,2048]{1,0:T(8,128)(2,1)}) fusion(f32[1024,2048]{1,0:T(8,128)} %reduce_sum.57, bf16[1024,2048]{1,0:T(8,128)(2,1)} %param.13), kind=kLoop, calls=%fused_computation.5 | loop fusion | flops 12581888 | bytes 16781312 | tf_op jit(solution)/shard_map/reduce_sum | solution.py:49
  273.9 135.7 %all-gather.8.cloned.1.call-done = bf16[2048,2816]{1,0:T(8,128)(2,1)} async-done(((bf16[64,2816]{1,0:T(8,128)(2,1)}), bf16[2048,2816]{1,0:T(8,128)(2,1)}) %all-gather.8.cloned.1.call-update) | async-done | bytes 11534352 | tf_op jit(solution)/shard_map/all_gather | solution.py:13
  409.6 11.9 %fusion.9 = f32[1024,1408]{1,0:T(8,128)} fusion(bf16[2048,2816]{1,0:T(8,128)(2,1)} %all-gather.8.cloned.1.call-done, bf16[1024,2048]{1,0:T(8,128)(2,1)} %get-tuple-element.6, f32[2048]{0:T(1024)S(1)} %convert_element_type.60, f32[1024]{0:T(1024)S(1)} %add_rsqrt_fusion.1), kind=kOutput, calls=%fused_computation.15 | convolution fusion | flops 5913968640 | bytes 15740928 | tf_op jit(solution)/shard_map/dot_general | solution.py:111
  421.5 147.9 %all-gather.10.cloned.1.call-done = bf16[1408,2048]{0,1:T(8,128)(2,1)} async-done(((bf16[1408,64]{0,1:T(8,128)(2,1)}), bf16[1408,2048]{0,1:T(8,128)(2,1)}) %all-gather.10.cloned.1.call-update) | async-done | bytes 5767184 | tf_op jit(solution)/shard_map/all_gather | solution.py:114
  569.4 20.9 %fusion.16 = bf16[1024,2048]{1,0:T(8,128)(2,1)} fusion(bf16[1408,2048]{0,1:T(8,128)(2,1)} %all-gather.10.cloned.1.call-done, f32[1024,1408]{1,0:T(8,128)} %fusion.9, bf16[2048,2816]{1,0:T(8,128)(2,1)} %all-gather.8.cloned.1.call-done, bf16[1024,2048]{1,0:T(8,128)(2,1)} %get-tuple-element.6, f32[2048]{0:T(1024)S(1)} %convert_element_type.60, ...), kind=kOutput, calls=%fused_computation.20 | convolution fusion | flops 11830296576 | bytes 25702400 | tf_op jit(solution)/shard_map/dot_general | solution.py:117
  590.3 28.2 %all_to_all.10 = bf16[2,512,2048]{2,1,0:T(8,128)(2,1)S(1)} all-to-all(bf16[2,512,2048]{2,1,0:T(8,128)(2,1)} %bitcast.29), channel_id=1, replica_groups=mesh['rep'=2,'fs'=32,'tp'=2] {'tp'}, dimensions={0} | all-to-all | bytes 8388608 | tf_op jit(solution)/shard_map/all_to_all | solution.py:43
  618.5 1.0 convert_reduce_fusion
  619.4 1.2 copy-done
  620.7 2.1 add_convert_fusion
  (20 shorter events, 0.1 us)
Async XLA Ops:
  6.5 13.4 %copy-start.5 = (bf16[2048]{0:T(1024)(128)(2,1)S(1)}, bf16[2048]{0:T(1024)(128)(2,1)}, u32[]{:S(2)}) copy-start(bf16[2048]{0:T(1024)(128)(2,1)} %param.14) | copy-start | bytes 12292
  6.5 13.5 %copy-start.9 = (bf16[4,128]{1,0:T(4,128)(2,1)S(1)}, bf16[4,128]{1,0:T(4,128)(2,1)}, u32[]{:S(2)}) copy-start(bf16[4,128]{1,0:T(4,128)(2,1)} %param.18) | copy-start | bytes 3076
  6.5 13.5 %copy-start.8 = (bf16[1024]{0:T(1024)(128)(2,1)S(1)}, bf16[1024]{0:T(1024)(128)(2,1)}, u32[]{:S(2)}) copy-start(bf16[1024]{0:T(1024)(128)(2,1)} %param.19) | copy-start | bytes 6148
  6.5 13.5 %copy-start.7 = (bf16[1024]{0:T(1024)(128)(2,1)S(1)}, bf16[1024]{0:T(1024)(128)(2,1)}, u32[]{:S(2)}) copy-start(bf16[1024]{0:T(1024)(128)(2,1)} %param.20) | copy-start | bytes 6148
  6.5 150.6 %all-gather.6.cloned.1.call-start = ((), (), s32[]{:S(2)}) async-start(), calls=%async_computation.2 | async-start | bytes 4325376 | tf_op jit(solution)/shard_map/all_gather | solution.py:13
  10.6 180.7 %all-to-all-start = ((bf16[32,512,64]{1,2,0:T(8,128)(2,1)}), bf16[32,512,64]{1,2,0:T(8,128)(2,1)}, u32[]{:S(2)}, u32[]{:S(2)}) async-start(bf16[32,512,64]{1,2,0:T(8,128)(2,1)} %broadcast_in_dim.13), calls=%async_computation | async-start | bytes 4194304 | tf_op jit(solution)/shard_map/all_to_all | solution.py:18
  19.9 234.4 %all-gather.12.cloned.1.call-start = ((), (), s32[]{:S(2)}) async-start(), calls=%async_computation.5 | async-start | bytes 25165824 | tf_op jit(solution)/shard_map/all_gather | solution.py:33
  183.8 1.6 copy-start.1
  185.4 1.1 copy-start.4
  202.9 0.9 copy-start.2
  202.9 1.0 copy-start.3
  202.9 2.4 copy-start.6
  202.9 206.7 %all-gather.8.cloned.1.call-start = ((), (), s32[]{:S(2)}) async-start(), calls=%async_computation.3 | async-start | bytes 11894784 | tf_op jit(solution)/shard_map/all_gather | solution.py:13
  204.7 364.7 %all-gather.10.cloned.1.call-start = ((), (), s32[]{:S(2)}) async-start(), calls=%async_computation.4 | async-start | bytes 5947392 | tf_op jit(solution)/shard_map/all_gather | solution.py:114
  618.5 2.2 copy-start
Sparse Core Ops, SparseCore 0:
  9.0 148.1 all-gather.5
  203.0 51.2 all-gather.11
  256.0 153.5 all-gather.7
  411.1 158.2 all-gather.9
where the time goes:
time: 630 us; the launch traced here: 629 us
  waiting for transfers between devices  467 us (74%)
  matrix products  51.8 us (8%)
  other arithmetic  44.6 us (7%)
  blocking collectives  28.2 us (4%)
  local copies, waits for them, and re-layouts  14.5 us (2%)
  between operations  13.3 us (2%)
  starting transfers between devices  9.5 us (2%)
    all_gather x2, waiting for transfers between devices, sent_together(): lax.all_gather(both, axis, axis=dim, tiled=True)  270 us
    all_gather x1, waiting for transfers between devices, on_device(): down_cols = lax.all_gather(w_down, 'fs', axis=1, tiled=True)  148 us
    all_gather x1, waiting for transfers between devices, total_of_pieces(): return lax.all_gather(x, axis).sum(0)  49.1 us
    all_to_all x1, blocking collectives, summed_on_arrival(): lax.all_to_all(pieces, axis, split_axis=0, concat_axis=0, tiled=True)  28.2 us
    dot_general x1, matrix products, on_device(): jnp.dot(hidden, down_cols, preferred_element_type=jnp.float32)  20.9 us
    reduce_sum x1, other arithmetic, spatial_unit(): spread = jnp.mean(jnp.square(active - center), axis=-1, keepdims=True)  14.4 us
  transfers between devices with their start and end apart: 5, of which 4 were waited for; matrix products, arithmetic and copies ran while one was open for 11% of the time, Pallas kernels for 0%

commit v1 on v0

--- a/solution.py
+++ b/solution.py
@@ -111,7 +111,9 @@
     gate = jnp.dot(normed_mid, gate_whole, preferred_element_type=jnp.float32)
     up = jnp.dot(normed_mid, up_whole, preferred_element_type=jnp.float32)
     hidden = (jax.nn.silu(gate) * up).astype(jnp.bfloat16)
-    down_cols = lax.all_gather(w_down, "fs", axis=1, tiled=True)
+    down_cols = jnp.concatenate(
+        lax.all_to_all(jnp.stack([w_down] * lax.axis_size("fs")), "fs", 0, 0), axis=1
+    )
     residual_rows = lax.dynamic_slice_in_dim(h_mid, row_start, half, 0).astype(jnp.float32)
     summed_rows = summed_on_arrival(
         jnp.dot(hidden, down_cols, preferred_element_type=jnp.float32).astype(jnp.bfloat16), "tp", 0

time: 630 us -> 497 us (0.79)
  waiting for transfers between devices: 467 us -> 330 us
    all_gather x1 -> x0, waiting for transfers between devices: 148 us -> none  [on_device(): down_cols = lax.all_gather(w_down, 'fs', axis=1, tiled=True)]
    all_gather x2, waiting for transfers between devices: 270 us -> 288 us  [sent_together(): lax.all_gather(both, axis, axis=dim, tiled=True)]
    all_gather x1, waiting for transfers between devices: 49.1 us -> 41.4 us  [total_of_pieces(): return lax.all_gather(x, axis).sum(0)]
  transfers between devices with their start and end apart: 5 -> 5, of which waited for: 4 -> 3; matrix products, arithmetic and copies ran while one was open for 11% -> 15% of each run, Pallas kernels for 0% -> 0%
where the time goes in v1:
time: 497 us
  waiting for transfers between devices  330 us (66%)
  matrix products  51.9 us (10%)
  other arithmetic  44.6 us (9%)
  blocking collectives  25 us (5%)
  local copies, waits for them, and re-layouts  17.8 us (4%)
  starting transfers between devices  14.5 us (3%)
  between operations  13.3 us (3%)
    all_gather x2, waiting for transfers between devices, sent_together(): lax.all_gather(both, axis, axis=dim, tiled=True)  288 us
    all_gather x1, waiting for transfers between devices, total_of_pieces(): return lax.all_gather(x, axis).sum(0)  41.4 us
    all_to_all x1, blocking collectives, summed_on_arrival(): lax.all_to_all(pieces, axis, split_axis=0, concat_axis=0, tiled=True)  25 us
    dot_general x1, matrix products, on_device(): jnp.dot(hidden, down_cols, preferred_element_type=jnp.float32)  20.9 us
    reduce_sum x1, other arithmetic, spatial_unit(): spread = jnp.mean(jnp.square(active - center), axis=-1, keepdims=True)  14.4 us
    dot_general x1, matrix products, on_device(): gate = jnp.dot(normed_mid, gate_whole, preferred_element_type=jnp.float32)  11.9 us
    reduce_sum x1, other arithmetic, total_of_pieces(): return lax.all_gather(x, axis).sum(0)  11.8 us
    dot_general x1, matrix products, on_device(): jnp.dot(gated, gathered_copies(w_mix_out, 'fs', 1), preferred_element_typ...  11.6 us
  transfers between devices with their start and end apart: 5, of which 3 were waited for; matrix products, arithmetic and copies ran while one was open for 15% of the time, Pallas kernels for 0%

profile of v1, /device:TPU:1, one launch (start us, length us, event | category | flops | bytes accessed | tf_op | source)
XLA Modules:
  0.0 496.8 jit_solution(9141011168080807351)
XLA Ops:
  6.5 0.0 all-gather.5.cloned.1.call-start
  6.6 1.6 pad_maximum_fusion.1
  8.1 0.0 all-gather.5.cloned.1.call-update
  8.2 2.4 broadcast_in_dim.13
  10.6 9.3 %all-to-all-start = ((bf16[32,512,64]{1,2,0:T(8,128)(2,1)}), bf16[32,512,64]{1,2,0:T(8,128)(2,1)}, u32[]{:S(2)}, u32[]{:S(2)}) async-start(bf16[32,512,64]{1,2,0:T(8,128)(2,1)} %broadcast_in_dim.13), calls=%async_computation | async-start | bytes 4194304 | tf_op jit(solution)/shard_map/all_to_all | solution.py:18
  19.9 0.0 all-gather.9.cloned.1.call-start
  20.0 0.0 copy-done.6
  20.0 0.0 copy-done.10
  20.0 0.1 dynamic-slice_convert_fusion
  20.1 3.1 fusion.3
  23.3 133.9 %all-gather.5.cloned.1.call-done = bf16[2048,1024]{1,0:T(8,128)(2,1)} async-done(((bf16[64,1024]{1,0:T(8,128)(2,1)}), bf16[2048,1024]{1,0:T(8,128)(2,1)}) %all-gather.5.cloned.1.call-update) | async-done | bytes 4194320 | tf_op jit(solution)/shard_map/all_gather | solution.py:13
  157.1 6.9 %fusion.35 = f32[1024,512]{1,0:T(8,128)} fusion(bf16[2048,1024]{1,0:T(8,128)(2,1)} %all-gather.5.cloned.1.call-done, bf16[1024,2048]{1,0:T(8,128)(2,1)} %param.13, f32[2048]{0:T(1024)S(1)} %convert_element_type.51, f32[1024]{0:T(1024)S(1)} %add_rsqrt_fusion.2), kind=kOutput, calls=%fused_computation.39 | convolution fusion | flops 2160066560 | bytes 8400896 | tf_op jit(solution)/shard_map/dot_general | solution.py:100
  164.1 2.6 reshape.66
  166.7 1.2 reduce_sum.55
  167.9 14.4 %multiply_reduce_fusion = f32[1024,2]{1,0:T(8,128)S(1)} fusion(f32[1024,2,256]{2,1,0:T(2,128)S(1)} %reshape.66, f32[1024,2]{1,0:T(8,128)S(1)} %broadcast_multiply_fusion), kind=kLoop, calls=%fused_computation.46 | loop fusion | flops 1570816 | bytes 2113536 | tf_op jit(solution)/shard_map/reduce_sum | solution.py:59
  182.3 0.1 add_rsqrt_fusion
  182.4 1.2 mul.112
  183.6 0.2 copy.33
  183.8 1.2 sub.17
  185.1 0.2 copy.32
  185.3 0.2 copy-done.1
  185.4 0.8 add_convert_fusion.1
  186.2 0.3 reshape.67
  186.5 0.5 bitcast_add_fusion
  187.1 2.4 copy.29
  189.5 1.8 copy.34
  191.2 0.0 all-to-all-done
  191.3 11.6 %fusion.51 = f32[1024,2048]{1,0:T(8,128)} fusion(bf16[512,2048]{0,1:T(8,128)(2,1)} %bitcast.5, f32[1024,512]{1,0:T(8,128)S(1)} %bitcast.33, bf16[2048,1024]{1,0:T(8,128)(2,1)} %all-gather.5.cloned.1.call-done, bf16[1024,2048]{1,0:T(8,128)(2,1)} %param.13, f32[2048]{0:T(1024)S(1)} %convert_element_type.51, f32[1024]{0:T(1024)S(1)} %add_rsqrt_fusion.2), kind=kOutput, calls=%fused_computation.47 | convolution fusion | flops 4308598784 | bytes 18886656 | tf_op jit(solution)/shard_map/dot_general | solution.py:104
  202.9 0.0 all-gather.9.cloned.1.call-update
  202.9 0.0 all-gather.7.cloned.1.call-start
  203.0 0.8 copy-done.3
  203.8 0.1 copy-done.4
  203.9 0.8 pad_maximum_fusion
  204.6 0.0 all-gather.7.cloned.1.call-update
  204.7 3.3 stack.2
  207.9 5.0 %all-to-all-start.1 = ((bf16[32,1408,64]{1,2,0:T(8,128)(2,1)}), bf16[32,1408,64]{1,2,0:T(8,128)(2,1)}, u32[]{:S(2)}, u32[]{:S(2)}) async-start(bf16[32,1408,64]{1,2,0:T(8,128)(2,1)} %stack.2), calls=%async_computation.1 | async-start | bytes 11534336 | tf_op jit(solution)/shard_map/all_to_all | solution.py:115
  213.0 0.0 copy-done.7
  213.0 41.4 %all-gather.9.cloned.1.call-done = f32[2048,2048]{1,0:T(8,128)} async-done(((f32[1024,2048]{1,0:T(8,128)}), f32[2048,2048]{1,0:T(8,128)}) %all-gather.9.cloned.1.call-update) | async-done | bytes 16777232 | tf_op jit(solution)/shard_map/all_gather | solution.py:33
  254.4 11.8 %reduce_sum.57 = f32[1024,2048]{1,0:T(8,128)} reduce(f32[2,1024,2048]{2,1,0:T(8,128)} %bitcast.26, f32[]{:T(128)} %constant.15.clone.1), dimensions={0}, to_apply=%region_3.4 | reduce | flops 2097152 | bytes 25165828 | tf_op jit(solution)/shard_map/reduce_sum | solution.py:33
  266.1 7.7 %fusion = (f32[1024]{0:T(1024)S(1)}, bf16[1024,2048]{1,0:T(8,128)(2,1)}) fusion(f32[1024,2048]{1,0:T(8,128)} %reduce_sum.57, bf16[1024,2048]{1,0:T(8,128)(2,1)} %param.13), kind=kLoop, calls=%fused_computation.5 | loop fusion | flops 12581888 | bytes 16781312 | tf_op jit(solution)/shard_map/reduce_sum | solution.py:49
  273.8 154.4 %all-gather.7.cloned.1.call-done = bf16[2048,2816]{1,0:T(8,128)(2,1)} async-done(((bf16[64,2816]{1,0:T(8,128)(2,1)}), bf16[2048,2816]{1,0:T(8,128)(2,1)}) %all-gather.7.cloned.1.call-update) | async-done | bytes 11534352 | tf_op jit(solution)/shard_map/all_gather | solution.py:13
  428.2 11.9 %fusion.9 = f32[1024,1408]{1,0:T(8,128)} fusion(bf16[2048,2816]{1,0:T(8,128)(2,1)} %all-gather.7.cloned.1.call-done, bf16[1024,2048]{1,0:T(8,128)(2,1)} %get-tuple-element.6, f32[2048]{0:T(1024)S(1)} %convert_element_type.60, f32[1024]{0:T(1024)S(1)} %add_rsqrt_fusion.1), kind=kOutput, calls=%fused_computation.15 | convolution fusion | flops 5913968640 | bytes 15740928 | tf_op jit(solution)/shard_map/dot_general | solution.py:111
  440.1 0.0 all-to-all-done.1
  440.1 20.9 %fusion.16 = bf16[1024,2048]{1,0:T(8,128)(2,1)} fusion(bf16[1408,2048]{0,1:T(8,128)(2,1)} %bitcast.8, f32[1024,1408]{1,0:T(8,128)} %fusion.9, bf16[2048,2816]{1,0:T(8,128)(2,1)} %all-gather.7.cloned.1.call-done, bf16[1024,2048]{1,0:T(8,128)(2,1)} %get-tuple-element.6, f32[2048]{0:T(1024)S(1)} %convert_element_type.60, f32[1024]{0:T(1024)S(1)} %add_rsqrt_fusion.1), kind=kOutput, calls=%fused_computation.20 | convolution fusion | flops 11830296576 | bytes 25702400 | tf_op jit(solution)/shard_map/dot_general | solution.py:119
  461.0 25.0 %all_to_all.15 = bf16[2,512,2048]{2,1,0:T(8,128)(2,1)S(1)} all-to-all(bf16[2,512,2048]{2,1,0:T(8,128)(2,1)} %bitcast.32), channel_id=1, replica_groups=mesh['rep'=2,'fs'=32,'tp'=2] {'tp'}, dimensions={0} | all-to-all | bytes 8388608 | tf_op jit(solution)/shard_map/all_to_all | solution.py:43
  486.0 1.0 convert_reduce_fusion
  487.0 1.2 copy-done
  488.2 2.1 add_convert_fusion
  (22 shorter events, 0.1 us)
Async XLA Ops:
  6.5 13.4 %copy-start.6 = (bf16[2048]{0:T(1024)(128)(2,1)S(1)}, bf16[2048]{0:T(1024)(128)(2,1)}, u32[]{:S(2)}) copy-start(bf16[2048]{0:T(1024)(128)(2,1)} %param.14) | copy-start | bytes 12292
  6.5 13.5 %copy-start.10 = (bf16[4,128]{1,0:T(4,128)(2,1)S(1)}, bf16[4,128]{1,0:T(4,128)(2,1)}, u32[]{:S(2)}) copy-start(bf16[4,128]{1,0:T(4,128)(2,1)} %param.18) | copy-start | bytes 3076
  6.5 13.5 %copy-start.9 = (bf16[1024]{0:T(1024)(128)(2,1)S(1)}, bf16[1024]{0:T(1024)(128)(2,1)}, u32[]{:S(2)}) copy-start(bf16[1024]{0:T(1024)(128)(2,1)} %param.19) | copy-start | bytes 6148
  6.5 13.5 %copy-start.8 = (bf16[1024]{0:T(1024)(128)(2,1)S(1)}, bf16[1024]{0:T(1024)(128)(2,1)}, u32[]{:S(2)}) copy-start(bf16[1024]{0:T(1024)(128)(2,1)} %param.20) | copy-start | bytes 6148
  6.5 150.6 %all-gather.5.cloned.1.call-start = ((), (), s32[]{:S(2)}) async-start(), calls=%async_computation.3 | async-start | bytes 4325376 | tf_op jit(solution)/shard_map/all_gather | solution.py:13
  10.6 180.7 %all-to-all-start = ((bf16[32,512,64]{1,2,0:T(8,128)(2,1)}), bf16[32,512,64]{1,2,0:T(8,128)(2,1)}, u32[]{:S(2)}, u32[]{:S(2)}) async-start(bf16[32,512,64]{1,2,0:T(8,128)(2,1)} %broadcast_in_dim.13), calls=%async_computation | async-start | bytes 4194304 | tf_op jit(solution)/shard_map/all_to_all | solution.py:18
  19.9 234.4 %all-gather.9.cloned.1.call-start = ((), (), s32[]{:S(2)}) async-start(), calls=%async_computation.5 | async-start | bytes 25165824 | tf_op jit(solution)/shard_map/all_gather | solution.py:33
  183.8 1.6 copy-start.1
  185.4 1.1 copy-start.5
  202.9 0.9 copy-start.3
  202.9 1.0 copy-start.4
  202.9 1.8 copy-start.2
  202.9 225.3 %all-gather.7.cloned.1.call-start = ((), (), s32[]{:S(2)}) async-start(), calls=%async_computation.4 | async-start | bytes 11894784 | tf_op jit(solution)/shard_map/all_gather | solution.py:13
  207.9 5.0 %copy-start.7 = (bf16[2048]{0:T(1024)(128)(2,1)S(1)}, bf16[2048]{0:T(1024)(128)(2,1)}, u32[]{:S(2)}) copy-start(bf16[2048]{0:T(1024)(128)(2,1)} %param.22) | copy-start | bytes 12292
  207.9 232.2 %all-to-all-start.1 = ((bf16[32,1408,64]{1,2,0:T(8,128)(2,1)}), bf16[32,1408,64]{1,2,0:T(8,128)(2,1)}, u32[]{:S(2)}, u32[]{:S(2)}) async-start(bf16[32,1408,64]{1,2,0:T(8,128)(2,1)} %stack.2), calls=%async_computation.1 | async-start | bytes 11534336 | tf_op jit(solution)/shard_map/all_to_all | solution.py:115
  486.0 2.2 copy-start
Sparse Core Ops, SparseCore 0:
  9.0 148.1 all-gather.4
  203.0 51.2 all-gather.8
  256.0 172.1 all-gather.6
